TPU v7x, 32 devices: a whole 2x2x4 slice. The times are simulated.
32 devices in a mesh: sp: 16 (over z, y, x), tp: 2 (over core).
Axes of the slice: x: 2, y: 2, z: 4, core: 2. Of those that a mesh axis runs over, the one named last changes fastest.
Arguments:
- query_proj: bfloat16 [4096, 1024], P('sp', 'tp'), may hold values from -6 to 6
- key_proj: bfloat16 [4096, 512], P('sp', 'tp'), may hold values from -6 to 6
- value_proj: bfloat16 [4096, 512], P('sp', 'tp'), may hold values from -6 to 6
- q_gain: float32 [64], replicated, may hold values from 1.1 to 10, as said below
- k_gain: float32 [64], replicated, may hold values from 1.1 to 10, as said below
- residual: bfloat16 [4096, 2048], P('sp'), may hold values from -6 to 6
- out_weight: bfloat16 [1024, 2048], P('tp'), may hold values from -0.75 to 0.75
- norm_gain: float32 [2048], replicated, may hold values from 0.1 to 1.9
- value_weight: bfloat16 [2048, 5120], P('sp', 'tp'), may hold values from -0.125 to 0.125
- gate_weight: bfloat16 [2048, 5120], P('sp', 'tp'), may hold values from -0.125 to 0.125
- down_weight: bfloat16 [5120, 2048], P('tp', 'sp'), may hold values from -0.078125 to 0.078125
- conv_value: float32 [3, 5120], P(None, 'tp'), may hold values from -3.5 to 3.5
- conv_gate: float32 [3, 5120], P(None, 'tp'), may hold values from -3.5 to 3.5
Outputs:
- layer_out: bfloat16 [4096, 2048], P(('sp', 'tp'))
Inputs may be any that keep to these rules, and one draw needn't show every extreme that they name: `q_gain`: per-dimension gains of the query norm. `k_gain`: per-dimension gains of the key norm.
All inputs are finite; a program needn't handle non-finite values.
Results may differ from a plain program's by a relative error of at most 0.015.
The roundings to bfloat16 on the way count: a program that leaves them out, or rounds other values in their place, can miss the bound.
Values may be sent and summed in bfloat16 or wider, within the bound.
A program may use at most 128 MiB of HBM per device.

v0:
```python
import functools
import math

import jax
import jax.numpy as jnp
from jax import lax
from jax.experimental import pallas as pl
from jax.experimental.pallas import tpu as pltpu
from jax.sharding import PartitionSpec as P


HEAD_DIM = 64
GRID_W = 64


NORM_EPS = 1e-06
ROPE_BASE = 10000.0


def rms_norm(block_in, gain_vec):
    values = block_in.astype(jnp.float32)
    inv_rms = lax.rsqrt(jnp.mean(values * values, axis=-1, keepdims=True) + NORM_EPS)
    return values * inv_rms * gain_vec


def rotate_half(values, position):
    full_width = values.shape[-1]
    half_width = full_width // 2
    frequency = ROPE_BASE ** (-jnp.arange(0, full_width, 2, dtype=jnp.float32) / full_width)
    angles = position.astype(jnp.float32)[:, None] * frequency[None, :]
    cosine = jnp.cos(angles)[:, None, :]
    sine_part = jnp.sin(angles)[:, None, :]
    first_half = values[..., :half_width]
    second_half = values[..., half_width:]
    return jnp.concatenate(
        [
            first_half * cosine - second_half * sine_part,
            first_half * sine_part + second_half * cosine,
        ],
        axis=-1,
    )


def grid_rotary(values, positions):
    half_width = values.shape[-1] // 2
    grid_row = positions // GRID_W
    column = positions % GRID_W
    return jnp.concatenate(
        [
            rotate_half(values[..., :half_width], grid_row),
            rotate_half(values[..., half_width:], column),
        ],
        axis=-1,
    )


def exchange_pieces(block_for, place, count, stride, axis_size):
    received = [block_for(place)]
    for hop in range(1, count):
        block = block_for((place + hop) % count)
        received.append(lax.ppermute(block, "sp", shifted(hop, count, stride, axis_size)))
    return received


def in_place_order(received, place):
    count = len(received)
    doubled = (received[::-1] * 2)[: 2 * count - 1]
    size = received[0].shape[0]
    whole = jnp.concatenate(doubled, axis=0)
    return lax.dynamic_slice_in_dim(whole, (count - 1 - place) * size, count * size, 0)


def shifted(hop, count, stride, axis_size):
    pairs = []
    for source in range(axis_size):
        group, rest = source // stride, source % stride
        pairs.append((source, ((group + hop) % count) * stride + rest))
    return pairs


def spread(block, count, stride):
    pieces = [block]
    for flip in range(1, stride):
        pairs = [
            (group * stride + rest, group * stride + (rest ^ flip))
            for group in range(count)
            for rest in range(stride)
        ]
        pieces.append(lax.ppermute(block, "sp", pairs))
    return pieces


def unflip(pieces, rest):
    bit = 1
    while bit < len(pieces):
        chosen = (rest & bit) != 0
        pieces = [
            jnp.where(chosen, pieces[at ^ bit], pieces[at]) for at in range(len(pieces))
        ]
        bit *= 2
    return pieces


def swap_cores(block):
    return lax.ppermute(block, "tp", [(0, 1), (1, 0)])


def attention_kernel(q_ref, k_ref, vt_ref, out_ref, *, span):
    queries = q_ref[...]
    rows, width = queries.shape
    run_max = jnp.full((1, rows), -1e30, jnp.float32)
    run_sum = jnp.zeros((1, rows), jnp.float32)
    run_acc = jnp.zeros((width, rows), jnp.float32)
    for start in range(0, k_ref.shape[0], span):
        scores = lax.dot_general(
            k_ref[start : start + span, :],
            queries,
            (((1,), (1,)), ((), ())),
            preferred_element_type=jnp.float32,
        )
        new_max = jnp.maximum(run_max, jnp.max(scores, axis=0, keepdims=True))
        probs = jnp.exp(scores - new_max)
        shrink = jnp.exp(run_max - new_max)
        run_sum = run_sum * shrink + jnp.sum(probs, axis=0, keepdims=True)
        run_acc = run_acc * shrink + jnp.dot(
            vt_ref[:, start : start + span],
            probs.astype(jnp.bfloat16),
            preferred_element_type=jnp.float32,
        )
        run_max = new_max
    out_ref[...] = (run_acc / run_sum).T.astype(jnp.bfloat16)


def attend(queries, keys, values_t):
    total, width = queries.shape
    key_count = keys.shape[0]
    block = math.gcd(total, 256)
    return pl.pallas_call(
        functools.partial(attention_kernel, span=math.gcd(key_count, 1024)),
        grid=(total // block,),
        out_shape=jax.ShapeDtypeStruct((total, width), jnp.bfloat16),
        in_specs=[
            pl.BlockSpec((block, width), lambda i: (i, 0)),
            pl.BlockSpec((key_count, width), lambda i: (0, 0)),
            pl.BlockSpec((width, key_count), lambda i: (0, 0)),
        ],
        out_specs=pl.BlockSpec((block, width), lambda i: (i, 0)),
        cost_estimate=pl.CostEstimate(
            flops=16 * total * key_count * width,
            bytes_accessed=4 * (total + key_count) * width,
            transcendentals=total * key_count,
        ),
    )(queries, keys, values_t)


def shards(
    query_proj,
    key_proj,
    value_proj,
    q_gain,
    k_gain,
    residual,
    out_weight,
    norm_gain,
    value_weight,
    gate_weight,
    down_weight,
    conv_value,
    conv_gate,
):
    tokens = query_proj.shape[0]
    heads_here = query_proj.shape[1] // HEAD_DIM
    kv_here = key_proj.shape[1] // HEAD_DIM
    group_size = heads_here // kv_here
    sp_size, tp_size = lax.axis_size("sp"), lax.axis_size("tp")
    count = math.gcd(sp_size, 4)
    stride = sp_size // count
    me, core = lax.axis_index("sp"), lax.axis_index("tp")
    place, rest = me // stride, me % stride
    positions = me * tokens + jnp.arange(tokens, dtype=jnp.int32)

    queries = grid_rotary(
        rms_norm(query_proj.reshape(tokens, heads_here, HEAD_DIM), q_gain), positions
    ) * HEAD_DIM ** (-0.5)
    queries = queries.astype(jnp.bfloat16)
    keys_rot = grid_rotary(
        rms_norm(key_proj.reshape(tokens, kv_here, HEAD_DIM), k_gain), positions
    ).astype(jnp.bfloat16)
    values = value_proj.reshape(tokens, kv_here, HEAD_DIM)

    ff_here = value_weight.shape[1]
    depth_here = value_weight.shape[0]
    hidden_here = ff_here // count

    split_heads = count if kv_here % count == 0 else 1
    kv_each = kv_here // split_heads
    packed = jnp.concatenate(
        [queries.reshape(tokens, kv_here, group_size * HEAD_DIM), keys_rot, values], axis=2
    ).transpose(1, 0, 2)
    packed = packed.reshape(split_heads, kv_each, tokens, (group_size + 2) * HEAD_DIM)
    if split_heads > 1:
        got = exchange_pieces(
            lambda at: lax.dynamic_index_in_dim(packed, at, 0, keepdims=False),
            place,
            count,
            stride,
            sp_size,
        )
        got, weights_in = lax.optimization_barrier((got, (value_weight, gate_weight, down_weight)))
    else:
        got, weights_in = [packed[0]], (value_weight, gate_weight, down_weight)
    value_in, gate_in, down_in = weights_in

    q_width = group_size * HEAD_DIM
    kv_mine = jnp.stack([piece[..., q_width:] for piece in got])
    if split_heads > 1:
        kv_all = jnp.stack(spread(kv_mine, count, stride))
    else:
        kv_all = lax.all_gather(kv_mine, "sp", axis=0)
    kv_all = kv_all.transpose(2 + 0, 0, 1, 3, 4).reshape(kv_each, sp_size * tokens, 2 * HEAD_DIM)

    def up_block(at):
        start = at * hidden_here
        return jnp.concatenate(
            [
                lax.dynamic_slice_in_dim(value_in, start, hidden_here, 1),
                lax.dynamic_slice_in_dim(gate_in, start, hidden_here, 1),
            ],
            axis=1,
        )

    def down_block(at):
        return lax.dynamic_slice_in_dim(down_in, at * hidden_here, hidden_here, 0)

    up_got = exchange_pieces(up_block, place, count, stride, sp_size)
    up_pieces = spread(in_place_order(up_got, place), count, stride)
    columns_here = down_weight.shape[1]
    down_got = exchange_pieces(down_block, place, count, stride, sp_size)
    down_cols = in_place_order(down_got, place).reshape(count, hidden_here, columns_here)
    down_cols = jnp.concatenate([down_cols[at] for at in range(count)], axis=1)
    down_pieces = spread(down_cols, count, stride)

    q_pieces = [piece[..., :q_width] for piece in got]
    per_head = []
    for kv_at in range(kv_each):
        keys_h = kv_all[kv_at, :, :HEAD_DIM]
        values_t = kv_all[kv_at, :, HEAD_DIM:].T
        per_group = []
        for group_at in range(group_size):
            columns = slice(group_at * HEAD_DIM, (group_at + 1) * HEAD_DIM)
            q_here = jnp.concatenate([piece[kv_at, :, columns] for piece in q_pieces], axis=0)
            per_group.append(attend(q_here, keys_h, values_t))
        per_head.append(jnp.concatenate(per_group, axis=1))
    done = jnp.concatenate(per_head, axis=1).reshape(len(got), tokens, -1)
    if split_heads > 1:
        back = [done[0]]
        for hop in range(1, count):
            back.append(lax.ppermute(done[hop], "sp", shifted(-hop, count, stride, sp_size)))
        attended = jnp.roll(jnp.stack(back), place, axis=0).transpose(1, 0, 2)
        attended = attended.reshape(tokens, heads_here * HEAD_DIM)
    else:
        attended = done[0]

    row_share = tokens // tp_size
    residual_mine = lax.dynamic_slice_in_dim(residual, core * row_share, row_share, 0)
    if tp_size == 2:
        weight_other = swap_cores(out_weight)
        halves = attended.reshape(2, row_share, heads_here * HEAD_DIM)
        rows_mine = lax.dynamic_index_in_dim(halves, core, 0, keepdims=False)
        rows_other = swap_cores(lax.dynamic_index_in_dim(halves, 1 - core, 0, keepdims=False))
        mix_mine = jnp.dot(rows_mine, out_weight, preferred_element_type=jnp.float32)
        mix_other = jnp.dot(rows_other, weight_other, preferred_element_type=jnp.float32)
        mix_out = (
            mix_mine.astype(jnp.bfloat16).astype(jnp.float32)
            + mix_other.astype(jnp.bfloat16).astype(jnp.float32)
        ).astype(jnp.bfloat16)
    else:
        mix_out = lax.psum_scatter(
            jnp.dot(attended, out_weight, preferred_element_type=jnp.float32).astype(jnp.bfloat16),
            "tp",
            scatter_dimension=0,
            tiled=True,
        )
    updated = (residual_mine.astype(jnp.float32) + mix_out.astype(jnp.float32)).astype(jnp.bfloat16)
    normed = rms_norm(updated, norm_gain).astype(jnp.bfloat16)
    width = normed.shape[1]
    normed = jnp.stack(
        [
            jnp.concatenate(
                [
                    normed[:, (at * stride + flip) * depth_here :][:, :depth_here]
                    for at in range(count)
                ],
                axis=1,
            )
            for flip in range(stride)
        ]
    )

    ups = []
    for hop in range(count):
        rows = normed
        if hop:
            rows = lax.ppermute(normed, "sp", shifted(hop, count, stride, sp_size))
        if tp_size == 2:
            other = swap_cores(rows)
            rows = jnp.concatenate(
                [jnp.where(core == 0, rows, other), jnp.where(core == 0, other, rows)], axis=1
            )
        else:
            rows = lax.all_gather(rows, "tp", axis=1, tiled=True)
        total = 0.0
        for flip in range(stride):
            part = lax.dynamic_index_in_dim(rows, rest ^ flip, 0, keepdims=False)
            total = total + jnp.dot(part, up_pieces[flip], preferred_element_type=jnp.float32)
        ups.append(total.astype(jnp.bfloat16))
    ups = jnp.stack(ups)

    forward = [
        (group * stride + at, group * stride + (at + 1) % stride)
        for group in range(count)
        for at in range(stride)
    ]
    backward = [(target, source) for source, target in forward]
    before = lax.ppermute(ups[:, -1], "sp", forward)
    after = lax.ppermute(ups[:, 0], "sp", backward)
    hops = jnp.arange(count)
    block_at = (place - hops) % count
    no_before = (rest == 0) & (block_at == 0)
    no_after = (rest == stride - 1) & (block_at == count - 1)
    before = jnp.where(rest == 0, jnp.roll(before, -1, axis=0), before)
    after = jnp.where(rest == stride - 1, jnp.roll(after, 1, axis=0), after)
    before = jnp.where(no_before[:, None], 0, before)
    after = jnp.where(no_after[:, None], 0, after)
    padded = jnp.concatenate([before[:, None], ups, after[:, None]], axis=1).astype(jnp.float32)
    taps = jnp.concatenate(
        [
            lax.dynamic_slice_in_dim(conv_value, place * hidden_here, hidden_here, 1),
            lax.dynamic_slice_in_dim(conv_gate, place * hidden_here, hidden_here, 1),
        ],
        axis=1,
    )
    conv = padded[:, :-2] * taps[0] + padded[:, 1:-1] * taps[1] + padded[:, 2:] * taps[2]
    hidden = (
        jax.nn.gelu(conv[..., hidden_here:], approximate=True) * conv[..., :hidden_here]
    ).astype(jnp.bfloat16)

    down_all = jnp.concatenate(down_pieces, axis=1)
    branch = 0.0
    for hop in list(range(1, count)) + [0]:
        partial = jnp.dot(hidden[hop], down_all, preferred_element_type=jnp.float32)
        if tp_size == 2:
            partial = partial.reshape(2, row_share, width)
            mine = lax.dynamic_index_in_dim(partial, core, 0, keepdims=False)
            theirs = lax.dynamic_index_in_dim(partial, 1 - core, 0, keepdims=False)
            other = swap_cores(theirs.astype(jnp.bfloat16))
            mine = mine + other.astype(jnp.float32)
        else:
            mine = lax.psum_scatter(
                partial.astype(jnp.bfloat16), "tp", scatter_dimension=0, tiled=True
            )
        if hop:
            mine = lax.ppermute(
                mine.astype(jnp.bfloat16), "sp", shifted(-hop, count, stride, sp_size)
            )
        branch = branch + mine.astype(jnp.float32)
    branch = branch.astype(jnp.bfloat16)
    span = count * columns_here
    pieces = unflip([branch[:, at * span : (at + 1) * span] for at in range(stride)], rest)
    branch = jnp.concatenate(
        [
            pieces[at][:, group * columns_here : (group + 1) * columns_here]
            for group in range(count)
            for at in range(stride)
        ],
        axis=1,
    )
    return (updated.astype(jnp.float32) + branch.astype(jnp.float32)).astype(jnp.bfloat16)


def fused_kernel(
    q_in, kv_in, res_in, wo_in, gain, wv_in, wg_in, wd_in, taps_v, taps_g, out,
    qraw, qhead, kvbuf, kbuf, vbuf, top, total, acc, att_send, att_all, wo, res, mix_send, mix_recv,
    own_mix, upd, rows, wup, wdown, ups, hidden, part_keep, part_send, part_recv, red_send,
    red_recv, fin, local_sem, send_sem, recv_sem,
):
    sp, core = lax.axis_index("sp"), lax.axis_index("tp")
    x, y, zl, zh = sp % 2, (sp // 2) % 2, (sp // 4) % 2, sp // 8
    fx, fy, fl, fh = 1 - 2 * x, 1 - 2 * y, 1 - 2 * zl, 1 - 2 * zh
    depth = wv_in.shape[0]
    ffs = wdown.shape[1]
    pairs, half, pair_w = out.shape
    tokens = 2 * half
    other = 1 - core

    def xs(flip):
        return x + fx * flip

    def mate(at):
        return sp + fx * (at % 2) + 4 * fl * (at // 2)

    def place(at):
        return xs(at % 2) + 2 * (zl + fl * (at // 2))

    mine = place(0)
    y_mate, z_mate = sp + 2 * fy, sp + 8 * fh
    diag_mate = sp + 2 * fy + 8 * fh

    def pair_at(rel):
        return (y + fy * (rel % 2)) + 2 * (zl + fl * ((rel // 2) % 2)) + 4 * (zh + fh * (rel // 4))

    ids = {}
    started = []

    def remote(name, src, dst, device):
        at = ids.setdefault(name, len(ids))
        assert at < send_sem.shape[0], len(ids)
        return pltpu.make_async_remote_copy(
            src_ref=src, dst_ref=dst, send_sem=send_sem.at[at], recv_sem=recv_sem.at[at],
            device_id=device, device_id_type=pl.DeviceIdType.MESH,
        )

    def send(name, src, dst, device):
        copy = remote(name, src, dst, device)
        copy.start()
        started.append(copy)

    def arrived(name, dst):
        remote(name, dst, dst, (sp, core)).wait_recv()

    def lanes(start, size):
        return pl.ds(pl.multiple_of(start, 128), size)

    barrier = pltpu.get_barrier_semaphore()
    partners = [(sp, other)] + [(mate(at), core) for at in (1, 2, 3)]
    partners += [(y_mate, core), (z_mate, core), (diag_mate, core)]
    for device in partners:
        pl.semaphore_signal(barrier, inc=1, device_id=device, device_id_type=pl.DeviceIdType.MESH)
    pl.semaphore_wait(barrier, len(partners))

    def piece(kind, rel, x_at):
        start = pl.multiple_of(x_at * depth, depth)
        if kind == "v":
            return wup.at[rel, pl.ds(start, depth), pl.ds(0, ffs)]
        if kind == "g":
            return wup.at[rel, pl.ds(start, depth), pl.ds(ffs, ffs)]
        return wdown.at[rel, :, pl.ds(start, depth)]

    def whole(kind, rel):
        if kind == "v":
            return wup.at[rel, :, pl.ds(0, ffs)]
        if kind == "g":
            return wup.at[rel, :, pl.ds(ffs, ffs)]
        return wdown.at[rel]

    def shard(kind, at):
        if kind == "d":
            return wd_in.at[pl.ds(pl.multiple_of(place(at) * ffs, 128), ffs), :]
        return (wv_in if kind == "v" else wg_in).at[:, lanes(place(at) * ffs, ffs)]

    def exchange(kind, at):
        send(f"w1{kind}{at}", shard(kind, at), piece(kind, 2 * (at // 2), x), (mate(at), core))

    def exchanged(kind, at):
        arrived(f"w1{kind}{at}", piece(kind, 2 * (at // 2), xs(at % 2)))

    def across(kind, at):
        src = piece(kind, 2 * (at // 2), xs(at % 2)) if at else shard(kind, 0)
        dst = piece(kind, 2 * (at // 2) + 4, xs(at % 2))
        send(f"wz{kind}{at}", src, dst, (z_mate, core))

    def crossed(kind, at):
        arrived(f"wz{kind}{at}", piece(kind, 2 * (at // 2) + 4, xs(at % 2)))

    def sideways(kind, rel):
        send(f"wy{kind}{rel}", whole(kind, rel), whole(kind, rel + 1), (y_mate, core))

    def from_side(kind, rel):
        arrived(f"wy{kind}{rel}", whole(kind, rel + 1))

    for at in (2, 3, 1):
        send(f"kv{at}", kv_in.at[place(at)], kvbuf.at[0, mine], (mate(at), core))
    for at in (2, 3, 1):
        send(f"q{at}", q_in.at[place(at)], qraw.at[mine], (mate(at), core))
    across("v", 0)
    locals_ = [
        pltpu.make_async_copy(shard(kind, 0), piece(kind, 0, x), local_sem.at[n])
        for n, kind in enumerate("vgd")
    ]
    locals_.append(pltpu.make_async_copy(wo_in, wo, local_sem.at[3]))
    locals_.append(
        pltpu.make_async_copy(
            res_in.at[pl.ds(pl.multiple_of(core * half, half), half), :], res, local_sem.at[4]
        )
    )
    for copy in locals_:
        copy.start()
    for kind in "vgd":
        exchange(kind, 1)
    qraw[mine] = q_in[mine]
    kvbuf[0, mine] = kv_in[mine]
    top[...] = jnp.full(top.shape, -1e30, jnp.float32)
    total[...] = jnp.zeros(total.shape, jnp.float32)
    acc[...] = jnp.zeros(acc.shape, jnp.float32)
    for at in (1, 2, 3):
        arrived(f"kv{at}", kvbuf.at[0, place(at)])
    send("kvz", kvbuf.at[0], kvbuf.at[2], (z_mate, core))
    send("kvy", kvbuf.at[0], kvbuf.at[1], (y_mate, core))
    for at in (2, 3):
        exchange("v", at)
    for at in (1, 2, 3):
        arrived(f"q{at}", qraw.at[place(at)])
    width = HEAD_DIM
    group = qraw.shape[2] // width
    blocks = qraw.shape[0]

    @pl.loop(0, blocks)
    def _(b):
        for a in range(group):
            qhead[b * group + a] = qraw[b][:, a * width : (a + 1) * width]

    def unpack(t):
        @pl.loop(0, blocks)
        def _(b):
            start = pl.multiple_of(b * tokens, tokens)
            pair = kvbuf[t, b]
            kbuf[t, pl.ds(start, tokens), :] = pair[:, :width]
            vbuf[t, :, pl.ds(start, tokens)] = pair[:, width:].T

    def attend_block(t, h):
        scores = lax.dot_general(
            kbuf[t], qhead[h], (((1,), (1,)), ((), ())), preferred_element_type=jnp.float32
        )
        old = top[h]
        new = jnp.maximum(old, jnp.max(scores, axis=0, keepdims=True))
        probs = jnp.exp(scores - new)
        shrink = jnp.exp(old - new)
        total[h] = total[h] * shrink + jnp.sum(probs, axis=0, keepdims=True)
        acc[h] = acc[h] * shrink + jnp.dot(
            vbuf[t], probs.astype(jnp.bfloat16), preferred_element_type=jnp.float32
        )
        top[h] = new

    def attend_some(t, lo, hi):
        @pl.loop(lo, hi)
        def _(h):
            attend_block(t, h)

    heads = blocks * group
    unpack(0)
    attend_some(0, 0, heads // 2)
    locals_[0].wait()
    locals_[1].wait()
    exchanged("v", 1)
    across("v", 1)
    sideways("v", 0)
    attend_some(0, heads // 2, heads)
    for at in (2, 3):
        exchange("g", at)
    arrived("kvy", kvbuf.at[1])
    unpack(1)
    attend_some(1, 0, heads)
    arrived("kvz", kvbuf.at[2])
    send("kvd", kvbuf.at[2], kvbuf.at[3], (y_mate, core))
    across("g", 0)
    exchanged("g", 1)
    sideways("g", 0)
    unpack(2)
    attend_some(2, 0, heads // 2)
    across("g", 1)
    for at in (2, 3):
        exchange("d", at)
    exchanged("v", 2)
    exchanged("v", 3)
    sideways("v", 2)
    attend_some(2, heads // 2, heads)
    arrived("kvd", kvbuf.at[3])
    unpack(3)

    def finish(block):
        first = block * group
        pieces = [acc[first + a] / total[first + a] for a in range(group)]
        return jnp.concatenate(pieces, axis=0).T.astype(jnp.bfloat16)

    for at in (2, 3, 1, 0):
        block = place(at)
        attend_some(3, block * group, block * group + group)
        if at:
            att_send[at - 1] = finish(block)
            send(f"att{at}", att_send.at[at - 1], att_all.at[mine], (mate(at), core))
        else:
            att_all[mine] = finish(block)
    across("v", 2)
    exchanged("g", 2)
    exchanged("g", 3)
    sideways("g", 2)
    locals_[3].wait()
    locals_[4].wait()
    for at in (1, 2, 3):
        arrived(f"att{at}", att_all.at[place(at)])

    def project(n, rows_at):
        start = pl.multiple_of(rows_at * half, half)
        left = jnp.concatenate([att_all[b, pl.ds(start, half), :] for b in range(blocks)], axis=1)
        return jnp.dot(left, wo[:, lanes(n * pair_w, pair_w)], preferred_element_type=jnp.float32)

    @pl.loop(0, pairs)
    def _(n):
        mix_send[n] = project(n, other).astype(jnp.bfloat16)

    send("mix", mix_send, mix_recv, (sp, other))

    @pl.loop(0, pairs)
    def _(n):
        own_mix[n] = project(n, core).astype(jnp.bfloat16)

    arrived("mix", mix_recv)

    def update(n, squares):
        mixed = own_mix[n].astype(jnp.float32) + mix_recv[n].astype(jnp.float32)
        mixed = mixed.astype(jnp.bfloat16).astype(jnp.float32)
        held = res[:, lanes(n * pair_w, pair_w)].astype(jnp.float32)
        new = (held + mixed).astype(jnp.bfloat16)
        upd[n] = new
        wide = new.astype(jnp.float32)
        return squares + jnp.sum(wide * wide, axis=1, keepdims=True)

    squares = lax.fori_loop(0, pairs, update, jnp.zeros((half, 1), jnp.float32))
    inv = lax.rsqrt(squares / (pairs * pair_w) + NORM_EPS)
    my_rows = pl.ds(pl.multiple_of(core * half, half), half)

    @pl.loop(0, pairs)
    def _(n):
        scaled = upd[n].astype(jnp.float32) * inv * gain[:, lanes(n * pair_w, pair_w)]
        rows[mine, n, my_rows, :] = scaled.astype(jnp.bfloat16)

    def rows_of(g, at):
        return rows.at[g, :, pl.ds(pl.multiple_of(at * half, half), half), :]

    send("row2", rows_of(mine, core), rows_of(mine, core), (mate(2), core))
    send("row1", rows_of(mine, core), rows_of(mine, core), (mate(1), core))
    send("row0", rows_of(mine, core), rows_of(mine, core), (sp, other))
    crossed("v", 0)
    crossed("v", 1)
    sideways("v", 4)
    across("v", 3)

    def up_dot(g, rels):
        left = jnp.concatenate([rows[g, pair_at(rel)] for rel in rels], axis=1)
        return left

    def up_block(g, rels, fresh):
        seg, x_at = g // 2, g % 2
        start = pl.multiple_of(8 + x_at * tokens, 8)
        left = up_dot(g, rels)

        @pl.loop(0, 2 * ffs // pair_w)
        def _(n):
            cols = lanes(n * pair_w, pair_w)
            part = jnp.zeros((tokens, pair_w), jnp.float32)
            for i, rel in enumerate(rels):
                part = part + jnp.dot(
                    left[:, i * pair_w : (i + 1) * pair_w], wup[rel, :, cols],
                    preferred_element_type=jnp.float32,
                )
            if fresh:
                ups[seg, pl.ds(start, tokens), cols] = part
            else:
                ups[seg, pl.ds(start, tokens), cols] += part

    for kind in "vg":
        from_side(kind, 0)
        from_side(kind, 2)
    arrived("row0", rows_of(mine, other))
    up_block(mine, (0, 2, 1, 3), True)
    across("g", 2)
    arrived("row2", rows_of(place(2), core))
    send("row3", rows_of(place(2), core), rows_of(place(2), core), (mate(1), core))
    send("fwd2", rows_of(place(2), core), rows_of(place(2), core), (sp, other))
    arrived("row1", rows_of(place(1), core))
    send("fwd1", rows_of(place(1), core), rows_of(place(1), core), (sp, other))
    crossed("g", 0)
    crossed("g", 1)
    sideways("g", 4)
    across("g", 3)
    arrived("fwd2", rows_of(place(2), other))
    up_block(place(2), (0, 2, 1, 3), True)
    arrived("fwd1", rows_of(place(1), other))
    up_block(place(1), (0, 2, 1, 3), True)
    locals_[2].wait()
    exchanged("d", 1)
    exchanged("d", 2)
    exchanged("d", 3)
    across("d", 0)
    arrived("row3", rows_of(place(3), core))
    send("fwd3", rows_of(place(3), core), rows_of(place(3), core), (sp, other))
    crossed("v", 2)
    crossed("v", 3)
    sideways("v", 6)
    across("d", 1)
    sideways("d", 0)
    arrived("fwd3", rows_of(place(3), other))
    up_block(place(3), (0, 2, 1, 3), True)
    crossed("g", 2)
    crossed("g", 3)
    sideways("g", 6)
    across("d", 2)
    across("d", 3)

    @pl.loop(0, blocks)
    def _(g):
        up_block(g, (4, 6), False)

    sideways("d", 2)
    for kind in "vg":
        from_side(kind, 4)
        from_side(kind, 6)

    @pl.loop(0, blocks)
    def _(g):
        up_block(g, (5, 7), False)

    span = 2 * tokens
    head, tail = pl.ds(8, 8), pl.ds(span, 8)
    before, after = pl.ds(0, 8), pl.ds(span + 8, 8)
    even = y == 0

    def edge(name, seg_from, rows_from, seg_to, rows_to, device):
        send_at = remote(name, ups.at[seg_from, rows_from, :], ups.at[seg_to, rows_to, :], device)
        return send_at

    @pl.when(even)
    def _():
        edge("h0", 1, head, 0, after, (y_mate, core)).start()
        edge("h1", 0, tail, 0, before, (y_mate, core)).start()
        edge("h2", 1, tail, 1, before, (y_mate, core)).start()

        @pl.when(zh == 1)
        def _():
            edge("h3", 0, head, 1, after, (diag_mate, core)).start()

        @pl.when(zh == 0)
        def _():
            ups[0, before, :] = jnp.zeros((8, 2 * ffs), jnp.float32)

    @pl.when(y == 1)
    def _():
        edge("h0", 0, head, 0, after, (y_mate, core)).start()
        edge("h1", 1, head, 1, after, (y_mate, core)).start()
        edge("h2", 0, tail, 1, before, (y_mate, core)).start()

        @pl.when(zh == 0)
        def _():
            edge("h3", 1, tail, 0, before, (diag_mate, core)).start()

        @pl.when(zh == 1)
        def _():
            ups[1, after, :] = jnp.zeros((8, 2 * ffs), jnp.float32)

    tap_cols = lanes(mine * ffs, ffs)
    tv, tg = taps_v[:, tap_cols], taps_g[:, tap_cols]
    step = 64

    def convolve(window, taps):
        rounded = window.astype(jnp.bfloat16).astype(jnp.float32)
        return (
            rounded[7 : 7 + step] * taps[0:1]
            + rounded[8 : 8 + step] * taps[1:2]
            + rounded[9 : 9 + step] * taps[2:3]
        )

    def hidden_block(i):
        seg, at = i // (span // step), i % (span // step)
        window = pl.ds(pl.multiple_of(at * step, 8), step + 16)
        for n in range(ffs // 128):
            left, right = slice(n * 128, n * 128 + 128), slice(ffs + n * 128, ffs + n * 128 + 128)
            conv_v = convolve(ups[seg, window, left], tv[:, left])
            conv_g = convolve(ups[seg, window, right], tg[:, left])
            value = jax.nn.gelu(conv_g, approximate=True) * conv_v
            hidden[pl.ds(pl.multiple_of(i * step, step), step), left] = value.astype(jnp.bfloat16)

    per = span // step

    @pl.loop(0, 2 * (per - 2))
    def _(i):
        seg = i // (per - 2)
        hidden_block(seg * per + 1 + i % (per - 2))

    @pl.when(even)
    def _():
        edge("h0", 0, head, 0, after, (sp, core)).wait_recv()
        edge("h1", 1, head, 1, after, (sp, core)).wait_recv()
        edge("h2", 0, tail, 1, before, (sp, core)).wait_recv()

        @pl.when(zh == 1)
        def _():
            edge("h3", 1, tail, 0, before, (sp, core)).wait_recv()

    @pl.when(y == 1)
    def _():
        edge("h0", 1, head, 0, after, (sp, core)).wait_recv()
        edge("h1", 0, tail, 0, before, (sp, core)).wait_recv()
        edge("h2", 1, tail, 1, before, (sp, core)).wait_recv()

        @pl.when(zh == 0)
        def _():
            edge("h3", 0, head, 1, after, (sp, core)).wait_recv()

    @pl.loop(0, 4)
    def _(i):
        hidden_block((i // 2) * per + (i % 2) * (per - 1))

    order = [0, 2, 1, 3, 4, 6, 5, 7]

    def down(rel):
        @pl.loop(0, blocks)
        def _(g):
            base = pl.multiple_of(g * tokens, tokens)
            theirs = hidden[pl.ds(pl.multiple_of(base + other * half, half), half), :]
            part_send[rel, g] = jnp.dot(
                theirs, wdown[rel], preferred_element_type=jnp.float32
            ).astype(jnp.bfloat16)

        send(f"part{rel}", part_send.at[rel], part_recv.at[rel], (sp, other))

        @pl.loop(0, blocks)
        def _(g):
            base = pl.multiple_of(g * tokens, tokens)
            ours = hidden[pl.ds(pl.multiple_of(base + core * half, half), half), :]
            part_keep[order.index(rel) % 2, g] = jnp.dot(ours, wdown[rel], preferred_element_type=jnp.float32)

    def merge(rel):
        arrived(f"part{rel}", part_recv.at[rel])
        for at in (2, 3, 1):
            g = place(at)
            both = part_keep[order.index(rel) % 2, g] + part_recv[rel, g].astype(jnp.float32)
            red_send[rel, at - 1] = both.astype(jnp.bfloat16)
            to = rel ^ (at & 2)
            send(f"red{to}{at}", red_send.at[rel, at - 1], red_recv.at[to, at - 1], (mate(at), core))
        fin[rel] = part_keep[order.index(rel) % 2, mine] + part_recv[rel, mine].astype(jnp.float32)

    def close(rel):
        branch = fin[rel]
        for at in (1, 2, 3):
            arrived(f"red{rel}{at}", red_recv.at[rel, at - 1])
            branch = branch + red_recv[rel, at - 1].astype(jnp.float32)
        n = pair_at(rel)
        wide = branch.astype(jnp.bfloat16).astype(jnp.float32)
        out[n] = (upd[n].astype(jnp.float32) + wide).astype(jnp.bfloat16)

    down(0)
    crossed("d", 0)
    crossed("d", 1)
    sideways("d", 4)
    for i, rel in enumerate(order[1:]):
        if rel == 1:
            from_side("d", 0)
        if rel == 3:
            from_side("d", 2)
        if rel == 6:
            crossed("d", 2)
            crossed("d", 3)
            sideways("d", 6)
        if rel == 5:
            from_side("d", 4)
        if rel == 7:
            from_side("d", 6)
        down(rel)
        merge(order[i])
        if i >= 3:
            close(order[i - 3])
    merge(order[-1])
    for rel in order[-4:]:
        close(rel)
    for copy in started:
        copy.wait_send()
    for name in ("h0", "h1", "h2"):
        edge(name, 0, head, 0, after, (sp, core)).wait_send()

    @pl.when((y + zh) == 1)
    def _():
        edge("h3", 0, head, 0, after, (sp, core)).wait_send()


def fused(q_pack, kv_pack, residual, out_weight, norm_gain, value_weight, gate_weight, down_weight,
          conv_value, conv_gate):
    groups, tokens, q_width = q_pack.shape
    half, width = tokens // 2, residual.shape[1]
    depth, ff_here = value_weight.shape
    pair_w = 2 * depth
    pairs = width // pair_w
    ffs = ff_here // groups
    heads = groups * (q_width // HEAD_DIM)
    keys = groups * tokens
    bf16, f32 = jnp.bfloat16, jnp.float32
    vmem, anywhere = pl.BlockSpec(memory_space=pltpu.VMEM), pl.BlockSpec(memory_space=pl.ANY)
    copies = 104
    return pl.pallas_call(
        fused_kernel,
        out_shape=jax.ShapeDtypeStruct((pairs, half, pair_w), bf16),
        in_specs=[vmem, vmem, anywhere, anywhere, vmem, anywhere, anywhere, anywhere, vmem, vmem],
        out_specs=vmem,
        scratch_shapes=[
            pltpu.VMEM((groups, tokens, q_width), bf16),
            pltpu.VMEM((heads, tokens, HEAD_DIM), bf16),
            pltpu.VMEM((4, groups, tokens, 2 * HEAD_DIM), bf16),
            pltpu.VMEM((4, keys, HEAD_DIM), bf16),
            pltpu.VMEM((4, HEAD_DIM, keys), bf16),
            pltpu.VMEM((heads, 1, tokens), f32),
            pltpu.VMEM((heads, 1, tokens), f32),
            pltpu.VMEM((heads, HEAD_DIM, tokens), f32),
            pltpu.VMEM((groups - 1, tokens, q_width), bf16),
            pltpu.VMEM((groups, tokens, q_width), bf16),
            pltpu.VMEM(out_weight.shape, bf16),
            pltpu.VMEM((half, width), bf16),
            pltpu.VMEM((pairs, half, pair_w), bf16),
            pltpu.VMEM((pairs, half, pair_w), bf16),
            pltpu.VMEM((pairs, half, pair_w), bf16),
            pltpu.VMEM((pairs, half, pair_w), bf16),
            pltpu.VMEM((groups, pairs, tokens, pair_w), bf16),
            pltpu.VMEM((pairs, pair_w, 2 * ffs), bf16),
            pltpu.VMEM((pairs, ffs, pair_w), bf16),
            pltpu.VMEM((2, 2 * tokens + 16, 2 * ffs), f32),
            pltpu.VMEM((keys, ffs), bf16),
            pltpu.VMEM((2, groups, half, pair_w), f32),
            pltpu.VMEM((pairs, groups, half, pair_w), bf16),
            pltpu.VMEM((pairs, groups, half, pair_w), bf16),
            pltpu.VMEM((pairs, groups - 1, half, pair_w), bf16),
            pltpu.VMEM((pairs, groups - 1, half, pair_w), bf16),
            pltpu.VMEM((pairs, half, pair_w), f32),
            pltpu.SemaphoreType.DMA((5,)),
            pltpu.SemaphoreType.DMA((copies,)),
            pltpu.SemaphoreType.DMA((copies,)),
        ],
        compiler_params=pltpu.CompilerParams(
            collective_id=0, has_side_effects=True, vmem_limit_bytes=60 * 2**20
        ),
    )(q_pack, kv_pack, residual, out_weight, norm_gain[None, :], value_weight, gate_weight,
      down_weight, conv_value, conv_gate)


def fused_layer(
    query_proj, key_proj, value_proj, q_gain, k_gain, residual, out_weight, norm_gain,
    value_weight, gate_weight, down_weight, conv_value, conv_gate,
):
    tokens = query_proj.shape[0]
    heads_here = query_proj.shape[1] // HEAD_DIM
    kv_here = key_proj.shape[1] // HEAD_DIM
    positions = lax.axis_index("sp") * tokens + jnp.arange(tokens, dtype=jnp.int32)
    queries = grid_rotary(
        rms_norm(query_proj.reshape(tokens, heads_here, HEAD_DIM), q_gain), positions
    ) * HEAD_DIM ** (-0.5)
    queries = queries.astype(jnp.bfloat16)
    keys_rot = grid_rotary(
        rms_norm(key_proj.reshape(tokens, kv_here, HEAD_DIM), k_gain), positions
    ).astype(jnp.bfloat16)
    values = value_proj.reshape(tokens, kv_here, HEAD_DIM)
    q_pack = queries.reshape(tokens, kv_here, -1).transpose(1, 0, 2)
    kv_pack = jnp.concatenate([keys_rot, values], axis=2).transpose(1, 0, 2)
    done = fused(q_pack, kv_pack, residual, out_weight, norm_gain, value_weight, gate_weight,
                 down_weight, conv_value, conv_gate)
    return done.transpose(1, 0, 2).reshape(tokens // 2, -1)


def fits(sp_size, tp_size, arrays):
    tokens, kv_here = arrays[0].shape[0], arrays[1].shape[1] // HEAD_DIM
    depth, ff_here = arrays[8].shape
    return (
        (sp_size, tp_size, kv_here) == (16, 2, 4)
        and depth % 128 == 0
        and ff_here % (kv_here * 128) == 0
        and (2 * ff_here // kv_here) % (2 * depth) == 0
        and tokens % 256 == 0
    )


def layer(*arrays):
    if fits(lax.axis_size("sp"), lax.axis_size("tp"), arrays):
        return fused_layer(*arrays)
    return shards(*arrays)


def solution(mesh):
    return jax.shard_map(
        layer,
        mesh=mesh,
        in_specs=(
            P("sp", "tp"),
            P("sp", "tp"),
            P("sp", "tp"),
            P(),
            P(),
            P("sp", None),
            P("tp", None),
            P(),
            P("sp", "tp"),
            P("sp", "tp"),
            P("tp", "sp"),
            P(None, "tp"),
            P(None, "tp"),
        ),
        out_specs=P(("sp", "tp"), None),
        check_vma=False,
    )
```

profile of v0, /device:TPU:14, one launch (start us, length us, event | category | flops | bytes accessed | tf_op | source)
XLA Modules:
  0.0 167.5 jit_solution(11927418388156107007)
XLA Ops:
  0.0 0.2 multiply_cosine_fusion.1
  0.2 0.1 copy.30
  0.3 0.1 copy.31
  0.4 0.1 copy.32
  0.5 0.1 copy.33
  0.6 1.0 copy.28
  1.6 0.1 copy.29
  1.8 0.9 multiply_multiply_fusion
  2.7 0.0 copy-start.1
  2.7 0.0 copy-start
  2.7 0.5 add_convert_fusion
  3.2 0.0 copy-start.2
  3.2 0.4 copy-done.1
  3.6 0.1 copy.34
  3.7 0.2 copy.35
  3.9 1.3 concatenate.10
  5.2 0.0 copy-done
  5.2 0.1 copy.26
  5.3 0.1 fusion
  5.4 0.0 copy-done.2
  5.4 0.1 fusion.1
  5.5 0.1 multiply_subtract_fusion.1
  5.6 0.8 copy.27
  6.5 158.7 %shard_map.127 = bf16[8,128,256]{2,1,0:T(8,128)(2,1)} custom-call(bf16[4,256,128]{2,1,0:T(8,128)(2,1)} %bitcast.18, bf16[4,256,128]{2,1,0:T(8,128)(2,1)} %bitcast.19, bf16[256,2048]{1,0:T(8,128)(2,1)} %res_in.1, bf16[512,2048]{1,0:T(8,128)(2,1)} %wo_in.1, f32[1,2048]{1,0:T(1,128)} %bitcast.21, bf16[128,2560]{1,0:T(8,128)(2,1)} %wv_in.1, ...), custom_call_target="tpu_custom_call" | custom-call | tf_op jit(solution)/shard_map/pallas_call | solution.py:898
  165.2 1.3 copy.36
  166.5 1.0 copy.37
  (6 shorter events, 0.1 us)
Async XLA Ops:
  2.7 0.9 copy-start.1
  2.7 2.4 %copy-start = (bf16[256,512]{1,0:T(8,128)(2,1)S(1)}, bf16[256,512]{1,0:T(8,128)(2,1)}, u32[]{:S(2)}) copy-start(bf16[256,512]{1,0:T(8,128)(2,1)} %param.13) | copy-start | bytes 786436
  3.2 2.1 %copy-start.2 = (f32[64]{0:T(128)S(1)}, f32[64]{0:T(128)}, u32[]{:S(2)}) copy-start(f32[64]{0:T(128)} %param.16) | copy-start | bytes 772
where the time goes:
time: 170 us; the launch traced here: 168 us
  Pallas kernels  159 us (94%)
  local copies, waits for them, and re-layouts  6.74 us (4%)
  other arithmetic  1.91 us (1%)
    pallas_call x1, Pallas kernels, fused(): pl.pallas_call(fused_kernel, out_shape=jax.ShapeDtypeStruct((pairs, half,...  159 us

commit v1 on v0

--- a/solution.py
+++ b/solution.py
@@ -389,7 +389,7 @@
     fx, fy, fl, fh = 1 - 2 * x, 1 - 2 * y, 1 - 2 * zl, 1 - 2 * zh
     depth = wv_in.shape[0]
     ffs = wdown.shape[1]
-    pairs, half, pair_w = out.shape
+    pairs, half, pair_w = upd.shape
     tokens = 2 * half
     other = 1 - core
 
@@ -458,16 +458,29 @@
             return wd_in.at[pl.ds(pl.multiple_of(place(at) * ffs, 128), ffs), :]
         return (wv_in if kind == "v" else wg_in).at[:, lanes(place(at) * ffs, ffs)]
 
-    def exchange(kind, at):
-        send(f"w1{kind}{at}", shard(kind, at), piece(kind, 2 * (at // 2), x), (mate(at), core))
+    def launch(name, src, dst, device, where):
+        fresh = name not in ids
+        copy = remote(name, src, dst, device)
+        if where is None:
+            copy.start()
+        else:
+            pl.when(where)(copy.start)
+        if fresh:
+            started.append(copy)
+
+    def exchange(kind, at, where=None):
+        dst = piece(kind, 2 * (at // 2), x)
+        launch(f"w1{kind}{at}", shard(kind, at), dst, (mate(at), core), where)
 
     def exchanged(kind, at):
         arrived(f"w1{kind}{at}", piece(kind, 2 * (at // 2), xs(at % 2)))
 
-    def across(kind, at):
+    inner, outer = zl != zh, zl == zh
+
+    def across(kind, at, where=None):
         src = piece(kind, 2 * (at // 2), xs(at % 2)) if at else shard(kind, 0)
         dst = piece(kind, 2 * (at // 2) + 4, xs(at % 2))
-        send(f"wz{kind}{at}", src, dst, (z_mate, core))
+        launch(f"wz{kind}{at}", src, dst, (z_mate, core), where)
 
     def crossed(kind, at):
         arrived(f"wz{kind}{at}", piece(kind, 2 * (at // 2) + 4, xs(at % 2)))
@@ -475,14 +488,21 @@
     def sideways(kind, rel):
         send(f"wy{kind}{rel}", whole(kind, rel), whole(kind, rel + 1), (y_mate, core))
 
+    def sideways_half(kind, at):
+        src = piece(kind, 0, xs(at)) if at else shard(kind, 0)
+        send(f"wy{kind}h{at}", src, piece(kind, 1, xs(at)), (y_mate, core))
+
     def from_side(kind, rel):
-        arrived(f"wy{kind}{rel}", whole(kind, rel + 1))
+        if rel or kind == "d":
+            arrived(f"wy{kind}{rel}", whole(kind, rel + 1))
+        else:
+            arrived(f"wy{kind}h0", piece(kind, 1, x))
+            arrived(f"wy{kind}h1", piece(kind, 1, xs(1)))
 
     for at in (2, 3, 1):
         send(f"kv{at}", kv_in.at[place(at)], kvbuf.at[0, mine], (mate(at), core))
     for at in (2, 3, 1):
         send(f"q{at}", q_in.at[place(at)], qraw.at[mine], (mate(at), core))
-    across("v", 0)
     locals_ = [
         pltpu.make_async_copy(shard(kind, 0), piece(kind, 0, x), local_sem.at[n])
         for n, kind in enumerate("vgd")
@@ -495,8 +515,6 @@
     )
     for copy in locals_:
         copy.start()
-    for kind in "vgd":
-        exchange(kind, 1)
     qraw[mine] = q_in[mine]
     kvbuf[0, mine] = kv_in[mine]
     top[...] = jnp.full(top.shape, -1e30, jnp.float32)
@@ -506,10 +524,15 @@
         arrived(f"kv{at}", kvbuf.at[0, place(at)])
     send("kvz", kvbuf.at[0], kvbuf.at[2], (z_mate, core))
     send("kvy", kvbuf.at[0], kvbuf.at[1], (y_mate, core))
-    for at in (2, 3):
+    across("v", 0)
+    sideways_half("v", 0)
+    for at in (1, 2, 3):
         exchange("v", at)
+    sideways_half("g", 0)
     for at in (1, 2, 3):
         arrived(f"q{at}", qraw.at[place(at)])
+    for at in (2, 3, 1):
+        exchange("g", at)
     width = HEAD_DIM
     group = qraw.shape[2] // width
     blocks = qraw.shape[0]
@@ -549,30 +572,29 @@
     heads = blocks * group
     unpack(0)
     attend_some(0, 0, heads // 2)
-    locals_[0].wait()
-    locals_[1].wait()
+    for copy in locals_[:3]:
+        copy.wait()
     exchanged("v", 1)
     across("v", 1)
-    sideways("v", 0)
+    sideways_half("v", 1)
+    across("g", 0)
     attend_some(0, heads // 2, heads)
-    for at in (2, 3):
-        exchange("g", at)
     arrived("kvy", kvbuf.at[1])
     unpack(1)
-    attend_some(1, 0, heads)
+    attend_some(1, 0, heads // 2)
+    exchanged("g", 1)
+    across("g", 1)
+    sideways_half("g", 1)
+    attend_some(1, heads // 2, heads)
     arrived("kvz", kvbuf.at[2])
     send("kvd", kvbuf.at[2], kvbuf.at[3], (y_mate, core))
-    across("g", 0)
-    exchanged("g", 1)
-    sideways("g", 0)
     unpack(2)
     attend_some(2, 0, heads // 2)
-    across("g", 1)
-    for at in (2, 3):
-        exchange("d", at)
     exchanged("v", 2)
     exchanged("v", 3)
     sideways("v", 2)
+    across("v", 2)
+    across("v", 3)
     attend_some(2, heads // 2, heads)
     arrived("kvd", kvbuf.at[3])
     unpack(3)
@@ -590,14 +612,17 @@
             send(f"att{at}", att_send.at[at - 1], att_all.at[mine], (mate(at), core))
         else:
             att_all[mine] = finish(block)
-    across("v", 2)
     exchanged("g", 2)
     exchanged("g", 3)
     sideways("g", 2)
-    locals_[3].wait()
-    locals_[4].wait()
+    exchange("d", 1)
+    for copy in locals_[3:]:
+        copy.wait()
     for at in (1, 2, 3):
         arrived(f"att{at}", att_all.at[place(at)])
+    crossed("v", 0)
+    crossed("v", 1)
+    sideways("v", 4)
 
     def project(n, rows_at):
         start = pl.multiple_of(rows_at * half, half)
@@ -640,16 +665,19 @@
     send("row2", rows_of(mine, core), rows_of(mine, core), (mate(2), core))
     send("row1", rows_of(mine, core), rows_of(mine, core), (mate(1), core))
     send("row0", rows_of(mine, core), rows_of(mine, core), (sp, other))
-    crossed("v", 0)
-    crossed("v", 1)
-    sideways("v", 4)
-    across("v", 3)
+    across("g", 2, outer)
+    across("g", 3, outer)
+    for at in (2, 3):
+        exchange("d", at, outer)
 
     def up_dot(g, rels):
         left = jnp.concatenate([rows[g, pair_at(rel)] for rel in rels], axis=1)
         return left
 
     def up_block(g, rels, fresh):
+        up_inner(g, rels, fresh)
+
+    def up_inner(g, rels, fresh):
         seg, x_at = g // 2, g % 2
         start = pl.multiple_of(8 + x_at * tokens, 8)
         left = up_dot(g, rels)
@@ -673,44 +701,47 @@
         from_side(kind, 2)
     arrived("row0", rows_of(mine, other))
     up_block(mine, (0, 2, 1, 3), True)
-    across("g", 2)
+    crossed("g", 0)
+    crossed("g", 1)
+    sideways("g", 4)
     arrived("row2", rows_of(place(2), core))
     send("row3", rows_of(place(2), core), rows_of(place(2), core), (mate(1), core))
     send("fwd2", rows_of(place(2), core), rows_of(place(2), core), (sp, other))
+    exchanged("d", 1)
+    sideways("d", 0)
     arrived("row1", rows_of(place(1), core))
     send("fwd1", rows_of(place(1), core), rows_of(place(1), core), (sp, other))
-    crossed("g", 0)
-    crossed("g", 1)
-    sideways("g", 4)
-    across("g", 3)
+    across("d", 0, outer)
+    across("d", 1, outer)
     arrived("fwd2", rows_of(place(2), other))
     up_block(place(2), (0, 2, 1, 3), True)
+    across("g", 2, inner)
+    across("g", 3, inner)
     arrived("fwd1", rows_of(place(1), other))
     up_block(place(1), (0, 2, 1, 3), True)
-    locals_[2].wait()
-    exchanged("d", 1)
-    exchanged("d", 2)
-    exchanged("d", 3)
-    across("d", 0)
-    arrived("row3", rows_of(place(3), core))
-    send("fwd3", rows_of(place(3), core), rows_of(place(3), core), (sp, other))
+    for at in (2, 3):
+        exchange("d", at, inner)
     crossed("v", 2)
     crossed("v", 3)
     sideways("v", 6)
-    across("d", 1)
-    sideways("d", 0)
+    arrived("row3", rows_of(place(3), core))
+    send("fwd3", rows_of(place(3), core), rows_of(place(3), core), (sp, other))
+    across("d", 0, inner)
+    across("d", 1, inner)
     arrived("fwd3", rows_of(place(3), other))
     up_block(place(3), (0, 2, 1, 3), True)
     crossed("g", 2)
     crossed("g", 3)
     sideways("g", 6)
-    across("d", 2)
-    across("d", 3)
 
     @pl.loop(0, blocks)
     def _(g):
         up_block(g, (4, 6), False)
 
+    exchanged("d", 2)
+    exchanged("d", 3)
+    across("d", 2)
+    across("d", 3)
     sideways("d", 2)
     for kind in "vg":
         from_side(kind, 4)
@@ -777,7 +808,9 @@
             conv_v = convolve(ups[seg, window, left], tv[:, left])
             conv_g = convolve(ups[seg, window, right], tg[:, left])
             value = jax.nn.gelu(conv_g, approximate=True) * conv_v
-            hidden[pl.ds(pl.multiple_of(i * step, step), step), left] = value.astype(jnp.bfloat16)
+            block, at_row = i // (tokens // step), (i % (tokens // step)) * step
+            to = (at_row // half) * blocks * half + block * half + at_row % half
+            hidden[pl.ds(pl.multiple_of(to, step), step), left] = value.astype(jnp.bfloat16)
 
     per = span // step
 
@@ -806,58 +839,86 @@
         def _():
             edge("h3", 0, head, 1, after, (sp, core)).wait_recv()
 
+    crossed("d", 0)
+    crossed("d", 1)
+    sideways("d", 4)
+
     @pl.loop(0, 4)
     def _(i):
         hidden_block((i // 2) * per + (i % 2) * (per - 1))
 
     order = [0, 2, 1, 3, 4, 6, 5, 7]
+    straight = order[-2:]
 
     def down(rel):
-        @pl.loop(0, blocks)
-        def _(g):
-            base = pl.multiple_of(g * tokens, tokens)
-            theirs = hidden[pl.ds(pl.multiple_of(base + other * half, half), half), :]
-            part_send[rel, g] = jnp.dot(
-                theirs, wdown[rel], preferred_element_type=jnp.float32
-            ).astype(jnp.bfloat16)
-
+        def product(at):
+            left = hidden[pl.ds(pl.multiple_of(at * blocks * half, half), blocks * half), :]
+            whole_part = jnp.dot(left, wdown[rel], preferred_element_type=jnp.float32)
+            return whole_part.reshape(blocks, half, pair_w)
+
+        part_send[rel] = product(other).astype(jnp.bfloat16)
         send(f"part{rel}", part_send.at[rel], part_recv.at[rel], (sp, other))
-
-        @pl.loop(0, blocks)
-        def _(g):
-            base = pl.multiple_of(g * tokens, tokens)
-            ours = hidden[pl.ds(pl.multiple_of(base + core * half, half), half), :]
-            part_keep[order.index(rel) % 2, g] = jnp.dot(ours, wdown[rel], preferred_element_type=jnp.float32)
+        part_keep[order.index(rel) % 2] = product(core)
 
     def merge(rel):
         arrived(f"part{rel}", part_recv.at[rel])
-        for at in (2, 3, 1):
+
+        def both(at):
             g = place(at)
-            both = part_keep[order.index(rel) % 2, g] + part_recv[rel, g].astype(jnp.float32)
-            red_send[rel, at - 1] = both.astype(jnp.bfloat16)
-            to = rel ^ (at & 2)
-            send(f"red{to}{at}", red_send.at[rel, at - 1], red_recv.at[to, at - 1], (mate(at), core))
-        fin[rel] = part_keep[order.index(rel) % 2, mine] + part_recv[rel, mine].astype(jnp.float32)
+            return part_keep[order.index(rel) % 2, g] + part_recv[rel, g].astype(jnp.float32)
+
+        if rel in straight:
+            for at in (2, 3, 1):
+                red_send[rel, at - 1] = both(at).astype(jnp.bfloat16)
+                to = across_rel(rel, at)
+                send(f"red{to}{at}", red_send.at[rel, at - 1], red_recv.at[to, at - 1],
+                     (mate(at), core))
+            fin[rel, 0] = both(0)
+            return
+        first, second = ways(rel)
+        for i, at in enumerate((first, 3)):
+            red_send[rel, i] = both(at).astype(jnp.bfloat16)
+        to = across_rel(rel, first)
+        send(f"reda{to}", red_send.at[rel, pl.ds(0, 2)], red_recv.at[to, pl.ds(0, 2)],
+             (mate(first), core))
+        fin[rel, 0] = both(0)
+        fin[rel, 1] = both(second)
+
+    def ways(rel):
+        return (1, 2) if rel < 4 and rel % 2 == 0 else (2, 1)
+
+    def across_rel(rel, at):
+        return rel ^ (at & 2)
+
+    def pass_on(rel):
+        second = ways(rel)[1]
+        arrived(f"reda{rel}", red_recv.at[rel, pl.ds(0, 2)])
+        red_send[rel, 2] = (fin[rel, 1] + red_recv[rel, 1].astype(jnp.float32)).astype(jnp.bfloat16)
+        to = across_rel(rel, second)
+        send(f"redb{to}", red_send.at[rel, 2], red_recv.at[to, 2], (mate(second), core))
 
     def close(rel):
-        branch = fin[rel]
-        for at in (1, 2, 3):
-            arrived(f"red{rel}{at}", red_recv.at[rel, at - 1])
-            branch = branch + red_recv[rel, at - 1].astype(jnp.float32)
+        branch = fin[rel, 0]
+        if rel in straight:
+            for at in (1, 2, 3):
+                arrived(f"red{rel}{at}", red_recv.at[rel, at - 1])
+                branch = branch + red_recv[rel, at - 1].astype(jnp.float32)
+        else:
+            arrived(f"redb{rel}", red_recv.at[rel, 2])
+            branch = branch + red_recv[rel, 0].astype(jnp.float32)
+            branch = branch + red_recv[rel, 2].astype(jnp.float32)
         n = pair_at(rel)
         wide = branch.astype(jnp.bfloat16).astype(jnp.float32)
-        out[n] = (upd[n].astype(jnp.float32) + wide).astype(jnp.bfloat16)
+        new = (upd[n].astype(jnp.float32) + wide).astype(jnp.bfloat16)
+        out[:, lanes(n * pair_w, pair_w)] = new
 
     down(0)
-    crossed("d", 0)
-    crossed("d", 1)
-    sideways("d", 4)
     for i, rel in enumerate(order[1:]):
         if rel == 1:
             from_side("d", 0)
         if rel == 3:
             from_side("d", 2)
-        if rel == 6:
+        if rel == 4:
             crossed("d", 2)
             crossed("d", 3)
             sideways("d", 6)
@@ -867,10 +928,11 @@
             from_side("d", 6)
         down(rel)
         merge(order[i])
-        if i >= 3:
-            close(order[i - 3])
+        if i >= 2:
+            pass_on(order[i - 2])
     merge(order[-1])
-    for rel in order[-4:]:
+    pass_on(order[-3])
+    for rel in order:
         close(rel)
     for copy in started:
         copy.wait_send()
@@ -897,7 +959,7 @@
     copies = 104
     return pl.pallas_call(
         fused_kernel,
-        out_shape=jax.ShapeDtypeStruct((pairs, half, pair_w), bf16),
+        out_shape=jax.ShapeDtypeStruct((half, width), bf16),
         in_specs=[vmem, vmem, anywhere, anywhere, vmem, anywhere, anywhere, anywhere, vmem, vmem],
         out_specs=vmem,
         scratch_shapes=[
@@ -927,7 +989,7 @@
             pltpu.VMEM((pairs, groups, half, pair_w), bf16),
             pltpu.VMEM((pairs, groups - 1, half, pair_w), bf16),
             pltpu.VMEM((pairs, groups - 1, half, pair_w), bf16),
-            pltpu.VMEM((pairs, half, pair_w), f32),
+            pltpu.VMEM((pairs, 2, half, pair_w), f32),
             pltpu.SemaphoreType.DMA((5,)),
             pltpu.SemaphoreType.DMA((copies,)),
             pltpu.SemaphoreType.DMA((copies,)),
@@ -957,9 +1019,8 @@
     values = value_proj.reshape(tokens, kv_here, HEAD_DIM)
     q_pack = queries.reshape(tokens, kv_here, -1).transpose(1, 0, 2)
     kv_pack = jnp.concatenate([keys_rot, values], axis=2).transpose(1, 0, 2)
-    done = fused(q_pack, kv_pack, residual, out_weight, norm_gain, value_weight, gate_weight,
+    return fused(q_pack, kv_pack, residual, out_weight, norm_gain, value_weight, gate_weight,
                  down_weight, conv_value, conv_gate)
-    return done.transpose(1, 0, 2).reshape(tokens // 2, -1)
 
 
 def fits(sp_size, tp_size, arrays):

time: 170 us -> 157 us (0.924)
  Pallas kernels: 159 us -> 147 us
    pallas_call x1, Pallas kernels: 159 us -> 147 us  [fused(): pl.pallas_call(fused_kernel, out_shape=jax.ShapeDtypeStruct((half, width)...]
    unnamed x9 -> x10, local copies, waits for them, and re-layouts: 1.62 us -> 3.5 us
where the time goes in v1:
time: 157 us; the launch traced here: 155 us
  Pallas kernels  147 us (94%)
  local copies, waits for them, and re-layouts  6.3 us (4%)
  other arithmetic  1.91 us (1%)
    pallas_call x1, Pallas kernels, fused(): pl.pallas_call(fused_kernel, out_shape=jax.ShapeDtypeStruct((half, width)...  147 us
    unnamed x10, local copies, waits for them, and re-layouts  3.5 us

profile of v1, /device:TPU:14, one launch (start us, length us, event | category | flops | bytes accessed | tf_op | source)
XLA Modules:
  0.0 155.2 jit_solution(1360341697713353345)
XLA Ops:
  0.0 0.2 multiply_cosine_fusion.1
  0.2 0.1 copy.28
  0.3 0.1 copy.29
  0.4 0.1 copy.30
  0.5 0.1 copy.31
  0.6 1.0 copy.26
  1.6 0.1 copy.27
  1.8 0.9 multiply_multiply_fusion
  2.7 0.0 copy-start.1
  2.7 0.0 copy-start
  2.7 0.5 add_convert_fusion
  3.2 0.0 copy-start.2
  3.2 0.4 copy-done.1
  3.6 0.1 copy.32
  3.7 0.2 copy.33
  3.9 1.3 concatenate.10
  5.2 0.0 copy-done
  5.2 0.1 copy.24
  5.3 0.1 fusion
  5.4 0.0 copy-done.2
  5.4 0.1 fusion.1
  5.5 0.1 multiply_subtract_fusion.1
  5.6 0.8 copy.25
  6.5 146.8 %shard_map.127 = bf16[128,2048]{1,0:T(8,128)(2,1)} custom-call(bf16[4,256,128]{2,1,0:T(8,128)(2,1)} %bitcast.14, bf16[4,256,128]{2,1,0:T(8,128)(2,1)} %bitcast.15, bf16[256,2048]{1,0:T(8,128)(2,1)} %res_in.1, bf16[512,2048]{1,0:T(8,128)(2,1)} %wo_in.1, f32[1,2048]{1,0:T(1,128)} %bitcast.17, bf16[128,2560]{1,0:T(8,128)(2,1)} %wv_in.1, ...), custom_call_target="tpu_custom_call" | custom-call | tf_op jit(solution)/shard_map/pallas_call | solution.py:960
  153.3 1.9 %copy.35 = bf16[128,2048]{1,0:T(8,128)(2,1)} copy(bf16[128,2048]{1,0:T(8,128)(2,1)} %shard_map.127) | data formatting | bytes 1048576
  (6 shorter events, 0.1 us)
Async XLA Ops:
  2.7 0.9 copy-start.1
  2.7 2.4 %copy-start = (bf16[256,512]{1,0:T(8,128)(2,1)S(1)}, bf16[256,512]{1,0:T(8,128)(2,1)}, u32[]{:S(2)}) copy-start(bf16[256,512]{1,0:T(8,128)(2,1)} %param.13) | copy-start | bytes 786436
  3.2 2.1 %copy-start.2 = (f32[64]{0:T(128)S(1)}, f32[64]{0:T(128)}, u32[]{:S(2)}) copy-start(f32[64]{0:T(128)} %param.16) | copy-start | bytes 772

commit v2 on v1

--- a/solution.py
+++ b/solution.py
@@ -3,6 +3,7 @@
 
 import jax
 import jax.numpy as jnp
+import numpy as np
 from jax import lax
 from jax.experimental import pallas as pl
 from jax.experimental.pallas import tpu as pltpu
@@ -379,8 +380,8 @@
 
 
 def fused_kernel(
-    q_in, kv_in, res_in, wo_in, gain, wv_in, wg_in, wd_in, taps_v, taps_g, out,
-    qraw, qhead, kvbuf, kbuf, vbuf, top, total, acc, att_send, att_all, wo, res, mix_send, mix_recv,
+    query, key, value, q_gain, k_gain, cosine, sine, res_in, wo_in, gain, wv_in, wg_in, wd_in, taps_v, taps_g, out,
+    q_in, kv_in, qraw, qhead, kvbuf, kbuf, vbuf, top, total, acc, att_send, att_all, wo, res, mix_send, mix_recv,
     own_mix, upd, rows, wup, wdown, ups, hidden, part_keep, part_send, part_recv, red_send,
     red_recv, fin, local_sem, send_sem, recv_sem,
 ):
@@ -436,6 +437,36 @@
     partners += [(y_mate, core), (z_mate, core), (diag_mate, core)]
     for device in partners:
         pl.semaphore_signal(barrier, inc=1, device_id=device, device_id_type=pl.DeviceIdType.MESH)
+
+    lane = lax.broadcasted_iota(jnp.int32, (tokens, 2 * HEAD_DIM), 1)
+    left_head = lane < HEAD_DIM
+    quarter = HEAD_DIM // 4
+    low = lane % (2 * quarter) < quarter
+    lanes_all = 2 * HEAD_DIM
+    q_row, k_row = (jnp.concatenate([ref[...], ref[...]], axis=1) for ref in (q_gain, k_gain))
+
+    def rotate(heads_pair, gain_row, scale):
+        wide = heads_pair.astype(jnp.float32)
+        squares = wide * wide
+        left = jnp.sum(jnp.where(left_head, squares, 0.0), axis=1, keepdims=True)
+        right = jnp.sum(jnp.where(left_head, 0.0, squares), axis=1, keepdims=True)
+        mean = jnp.where(left_head, left, right) / HEAD_DIM
+        normed = wide * lax.rsqrt(mean + NORM_EPS) * gain_row
+        swapped = jnp.where(
+            low,
+            pltpu.roll(normed, lanes_all - quarter, 1),
+            pltpu.roll(normed, quarter, 1),
+        )
+        return (normed * cosine[...] + swapped * sine[...]) * scale
+
+    for m in range(key.shape[1] // lanes_all):
+        cols = slice(m * lanes_all, (m + 1) * lanes_all)
+        turned = rotate(key[:, cols], k_row, 1.0)
+        passed = value[:, cols].astype(jnp.float32)
+        first = jnp.where(left_head, turned, pltpu.roll(passed, HEAD_DIM, 1))
+        second = jnp.where(left_head, pltpu.roll(turned, HEAD_DIM, 1), passed)
+        kv_in[2 * m] = first.astype(jnp.bfloat16)
+        kv_in[2 * m + 1] = second.astype(jnp.bfloat16)
     pl.semaphore_wait(barrier, len(partners))
 
     def piece(kind, rel, x_at):
@@ -485,8 +516,8 @@
     def crossed(kind, at):
         arrived(f"wz{kind}{at}", piece(kind, 2 * (at // 2) + 4, xs(at % 2)))
 
-    def sideways(kind, rel):
-        send(f"wy{kind}{rel}", whole(kind, rel), whole(kind, rel + 1), (y_mate, core))
+    def sideways(kind, rel, where=None):
+        launch(f"wy{kind}{rel}", whole(kind, rel), whole(kind, rel + 1), (y_mate, core), where)
 
     def sideways_half(kind, at):
         src = piece(kind, 0, xs(at)) if at else shard(kind, 0)
@@ -501,6 +532,9 @@
 
     for at in (2, 3, 1):
         send(f"kv{at}", kv_in.at[place(at)], kvbuf.at[0, mine], (mate(at), core))
+    for m in range(q_in.shape[0]):
+        cols = slice(m * lanes_all, (m + 1) * lanes_all)
+        q_in[m] = rotate(query[:, cols], q_row, HEAD_DIM ** (-0.5)).astype(jnp.bfloat16)
     for at in (2, 3, 1):
         send(f"q{at}", q_in.at[place(at)], qraw.at[mine], (mate(at), core))
     locals_ = [
@@ -524,13 +558,13 @@
         arrived(f"kv{at}", kvbuf.at[0, place(at)])
     send("kvz", kvbuf.at[0], kvbuf.at[2], (z_mate, core))
     send("kvy", kvbuf.at[0], kvbuf.at[1], (y_mate, core))
+    sideways_half("v", 0)
+    for at in (1, 2, 3):
+        arrived(f"q{at}", qraw.at[place(at)])
     across("v", 0)
-    sideways_half("v", 0)
     for at in (1, 2, 3):
         exchange("v", at)
     sideways_half("g", 0)
-    for at in (1, 2, 3):
-        arrived(f"q{at}", qraw.at[place(at)])
     for at in (2, 3, 1):
         exchange("g", at)
     width = HEAD_DIM
@@ -659,16 +693,20 @@
         scaled = upd[n].astype(jnp.float32) * inv * gain[:, lanes(n * pair_w, pair_w)]
         rows[mine, n, my_rows, :] = scaled.astype(jnp.bfloat16)
 
-    def rows_of(g, at):
-        return rows.at[g, :, pl.ds(pl.multiple_of(at * half, half), half), :]
-
-    send("row2", rows_of(mine, core), rows_of(mine, core), (mate(2), core))
-    send("row1", rows_of(mine, core), rows_of(mine, core), (mate(1), core))
-    send("row0", rows_of(mine, core), rows_of(mine, core), (sp, other))
+    def rows_of(g, at, part=None):
+        cut = slice(None) if part is None else pl.ds(part * (pairs // 2), pairs // 2)
+        return rows.at[g, cut, pl.ds(pl.multiple_of(at * half, half), half), :]
+
+    def spread_rows(name, at_block, device, part=None):
+        ref = rows_of(place(at_block), core, part)
+        send(name, ref, ref, device)
+
+    for part in (0, 1):
+        spread_rows(f"row2{part}", 0, (mate(2), core), part)
+        spread_rows(f"row1{1 - part}", 0, (mate(1), core), 1 - part)
+    spread_rows("row0", 0, (sp, other))
     across("g", 2, outer)
     across("g", 3, outer)
-    for at in (2, 3):
-        exchange("d", at, outer)
 
     def up_dot(g, rels):
         left = jnp.concatenate([rows[g, pair_at(rel)] for rel in rels], axis=1)
@@ -704,28 +742,34 @@
     crossed("g", 0)
     crossed("g", 1)
     sideways("g", 4)
-    arrived("row2", rows_of(place(2), core))
-    send("row3", rows_of(place(2), core), rows_of(place(2), core), (mate(1), core))
-    send("fwd2", rows_of(place(2), core), rows_of(place(2), core), (sp, other))
+    arrived("row20", rows_of(place(2), core, 0))
+    spread_rows("row30", 2, (mate(1), core), 0)
+    arrived("row11", rows_of(place(1), core, 1))
+    spread_rows("row31", 1, (mate(2), core), 1)
     exchanged("d", 1)
-    sideways("d", 0)
-    arrived("row1", rows_of(place(1), core))
-    send("fwd1", rows_of(place(1), core), rows_of(place(1), core), (sp, other))
     across("d", 0, outer)
     across("d", 1, outer)
+    for at in (2, 3):
+        exchange("d", at, outer)
+    arrived("row21", rows_of(place(2), core, 1))
+    spread_rows("fwd2", 2, (sp, other))
+    arrived("row10", rows_of(place(1), core, 0))
+    spread_rows("fwd1", 1, (sp, other))
+    sideways("d", 0)
     arrived("fwd2", rows_of(place(2), other))
     up_block(place(2), (0, 2, 1, 3), True)
-    across("g", 2, inner)
-    across("g", 3, inner)
-    arrived("fwd1", rows_of(place(1), other))
-    up_block(place(1), (0, 2, 1, 3), True)
-    for at in (2, 3):
-        exchange("d", at, inner)
     crossed("v", 2)
     crossed("v", 3)
     sideways("v", 6)
-    arrived("row3", rows_of(place(3), core))
-    send("fwd3", rows_of(place(3), core), rows_of(place(3), core), (sp, other))
+    across("g", 2, inner)
+    across("g", 3, inner)
+    for at in (2, 3):
+        exchange("d", at, inner)
+    arrived("fwd1", rows_of(place(1), other))
+    up_block(place(1), (0, 2, 1, 3), True)
+    arrived("row30", rows_of(place(3), core, 0))
+    arrived("row31", rows_of(place(3), core, 1))
+    spread_rows("fwd3", 3, (sp, other))
     across("d", 0, inner)
     across("d", 1, inner)
     arrived("fwd3", rows_of(place(3), other))
@@ -738,14 +782,18 @@
     def _(g):
         up_block(g, (4, 6), False)
 
-    exchanged("d", 2)
-    exchanged("d", 3)
-    across("d", 2)
-    across("d", 3)
-    sideways("d", 2)
+    @pl.when(inner)
+    def _():
+        exchanged("d", 2)
+        exchanged("d", 3)
+
+    across("d", 2, inner)
+    across("d", 3, inner)
+    sideways("d", 2, inner)
     for kind in "vg":
         from_side(kind, 4)
         from_side(kind, 6)
+
 
     @pl.loop(0, blocks)
     def _(g):
@@ -839,6 +887,14 @@
         def _():
             edge("h3", 0, head, 1, after, (sp, core)).wait_recv()
 
+    @pl.when(outer)
+    def _():
+        exchanged("d", 2)
+        exchanged("d", 3)
+
+    across("d", 2, outer)
+    across("d", 3, outer)
+    sideways("d", 2, outer)
     crossed("d", 0)
     crossed("d", 1)
     sideways("d", 4)
@@ -848,7 +904,7 @@
         hidden_block((i // 2) * per + (i % 2) * (per - 1))
 
     order = [0, 2, 1, 3, 4, 6, 5, 7]
-    straight = order[-2:]
+    straight = order[-4:]
 
     def down(rel):
         def product(at):
@@ -875,7 +931,7 @@
                      (mate(at), core))
             fin[rel, 0] = both(0)
             return
-        first, second = ways(rel)
+        first, second = ways()
         for i, at in enumerate((first, 3)):
             red_send[rel, i] = both(at).astype(jnp.bfloat16)
         to = across_rel(rel, first)
@@ -884,14 +940,14 @@
         fin[rel, 0] = both(0)
         fin[rel, 1] = both(second)
 
-    def ways(rel):
-        return (1, 2) if rel < 4 and rel % 2 == 0 else (2, 1)
+    def ways():
+        return (1, 2)
 
     def across_rel(rel, at):
         return rel ^ (at & 2)
 
     def pass_on(rel):
-        second = ways(rel)[1]
+        second = ways()[1]
         arrived(f"reda{rel}", red_recv.at[rel, pl.ds(0, 2)])
         red_send[rel, 2] = (fin[rel, 1] + red_recv[rel, 1].astype(jnp.float32)).astype(jnp.bfloat16)
         to = across_rel(rel, second)
@@ -928,10 +984,9 @@
             from_side("d", 6)
         down(rel)
         merge(order[i])
-        if i >= 2:
+        if i >= 2 and order[i - 2] not in straight:
             pass_on(order[i - 2])
     merge(order[-1])
-    pass_on(order[-3])
     for rel in order:
         close(rel)
     for copy in started:
@@ -944,9 +999,10 @@
         edge("h3", 0, head, 0, after, (sp, core)).wait_send()
 
 
-def fused(q_pack, kv_pack, residual, out_weight, norm_gain, value_weight, gate_weight, down_weight,
-          conv_value, conv_gate):
-    groups, tokens, q_width = q_pack.shape
+def fused(query_proj, key_proj, value_proj, gains, tables, residual, out_weight, norm_gain,
+          value_weight, gate_weight, down_weight, conv_value, conv_gate):
+    groups, tokens = key_proj.shape[1] // HEAD_DIM, query_proj.shape[0]
+    q_width = query_proj.shape[1] // groups
     half, width = tokens // 2, residual.shape[1]
     depth, ff_here = value_weight.shape
     pair_w = 2 * depth
@@ -960,9 +1016,11 @@
     return pl.pallas_call(
         fused_kernel,
         out_shape=jax.ShapeDtypeStruct((half, width), bf16),
-        in_specs=[vmem, vmem, anywhere, anywhere, vmem, anywhere, anywhere, anywhere, vmem, vmem],
+        in_specs=[vmem] * 7 + [anywhere, anywhere, vmem, anywhere, anywhere, anywhere, vmem, vmem],
         out_specs=vmem,
         scratch_shapes=[
+            pltpu.VMEM((groups, tokens, q_width), bf16),
+            pltpu.VMEM((groups, tokens, 2 * HEAD_DIM), bf16),
             pltpu.VMEM((groups, tokens, q_width), bf16),
             pltpu.VMEM((heads, tokens, HEAD_DIM), bf16),
             pltpu.VMEM((4, groups, tokens, 2 * HEAD_DIM), bf16),
@@ -997,7 +1055,7 @@
         compiler_params=pltpu.CompilerParams(
             collective_id=0, has_side_effects=True, vmem_limit_bytes=60 * 2**20
         ),
-    )(q_pack, kv_pack, residual, out_weight, norm_gain[None, :], value_weight, gate_weight,
+    )(query_proj, key_proj, value_proj, *gains, *tables, residual, out_weight, norm_gain[None, :], value_weight, gate_weight,
       down_weight, conv_value, conv_gate)
 
 
@@ -1005,22 +1063,20 @@
     query_proj, key_proj, value_proj, q_gain, k_gain, residual, out_weight, norm_gain,
     value_weight, gate_weight, down_weight, conv_value, conv_gate,
 ):
-    tokens = query_proj.shape[0]
-    heads_here = query_proj.shape[1] // HEAD_DIM
-    kv_here = key_proj.shape[1] // HEAD_DIM
-    positions = lax.axis_index("sp") * tokens + jnp.arange(tokens, dtype=jnp.int32)
-    queries = grid_rotary(
-        rms_norm(query_proj.reshape(tokens, heads_here, HEAD_DIM), q_gain), positions
-    ) * HEAD_DIM ** (-0.5)
-    queries = queries.astype(jnp.bfloat16)
-    keys_rot = grid_rotary(
-        rms_norm(key_proj.reshape(tokens, kv_here, HEAD_DIM), k_gain), positions
-    ).astype(jnp.bfloat16)
-    values = value_proj.reshape(tokens, kv_here, HEAD_DIM)
-    q_pack = queries.reshape(tokens, kv_here, -1).transpose(1, 0, 2)
-    kv_pack = jnp.concatenate([keys_rot, values], axis=2).transpose(1, 0, 2)
-    return fused(q_pack, kv_pack, residual, out_weight, norm_gain, value_weight, gate_weight,
-                 down_weight, conv_value, conv_gate)
+    tokens, width = query_proj.shape[0], 2 * HEAD_DIM
+    positions = lax.axis_index("sp") * tokens + lax.broadcasted_iota(jnp.int32, (tokens, width), 0)
+    lane = lax.broadcasted_iota(jnp.int32, (tokens, width), 1)
+    half = HEAD_DIM // 2
+    frequency = ROPE_BASE ** (-np.arange(0, half, 2, dtype=np.float32) / half)
+    frequency = np.tile(frequency.astype(np.float32), width // (half // 2))[None, :]
+    in_first = lane % HEAD_DIM < half
+    place = jnp.where(in_first, positions // GRID_W, positions % GRID_W)
+    angle = place.astype(jnp.float32) * frequency
+    sign = jnp.where(lane % half < half // 2, -1.0, 1.0)
+    tables = (jnp.cos(angle), jnp.sin(angle) * sign)
+    gains = (q_gain[None, :], k_gain[None, :])
+    return fused(query_proj, key_proj, value_proj, gains, tables, residual, out_weight, norm_gain,
+                 value_weight, gate_weight, down_weight, conv_value, conv_gate)
 
 
 def fits(sp_size, tp_size, arrays):
@@ -1029,6 +1085,7 @@
     return (
         (sp_size, tp_size, kv_here) == (16, 2, 4)
         and depth % 128 == 0
+        and arrays[0].shape[1] == 2 * arrays[1].shape[1]
         and ff_here % (kv_here * 128) == 0
         and (2 * ff_here // kv_here) % (2 * depth) == 0
         and tokens % 256 == 0

time: 157 us -> 148 us (0.943); the launches traced: 155 us -> 148 us
  local copies, waits for them, and re-layouts: 6.3 us -> 1.88 us
  Pallas kernels: 147 us -> 144 us
    pallas_call x1, Pallas kernels: 147 us -> 144 us  [fused(): pl.pallas_call(fused_kernel, out_shape=jax.ShapeDtypeStruct((half, width)...]
    unnamed x10 -> x1, local copies, waits for them, and re-layouts: 3.5 us -> 1.88 us
where the time goes in v2:
time: 148 us
  Pallas kernels  144 us (97%)
  other arithmetic  2.15 us (1%)
  local copies, waits for them, and re-layouts  1.88 us (1%)
    pallas_call x1, Pallas kernels, fused(): pl.pallas_call(fused_kernel, out_shape=jax.ShapeDtypeStruct((half, width)...  144 us

profile of v2, /device:TPU:14, one launch (start us, length us, event | category | flops | bytes accessed | tf_op | source)
XLA Modules:
  0.0 148.3 jit_solution(18358743506403728770)
XLA Ops:
  0.1 2.1 %select_multiply_fusion = (f32[256,128]{1,0:T(8,128)}, f32[256,128]{1,0:T(8,128)}) fusion(s32[128]{0:T(128)S(1)} %get-tuple-element.15, s32[128]{0:T(128)S(1)} %get-tuple-element.17, f32[128]{0:T(128)} %constant.68, s32[256]{0:T(256)S(1)} %get-tuple-element.10, s32[256]{0:T(256)S(1)} %get-tuple-element.11, s32[256]{0:T(256)S(1)} %get-tuple-element.9, ...), kind=kLoop, calls=%fused_computation | loop fusion | flops 360448 | bytes 269568 | tf_op jit(solution)/shard_map/mul | solution.py:1076
  2.2 144.2 %shard_map.136 = bf16[128,2048]{1,0:T(8,128)(2,1)} custom-call(bf16[256,512]{1,0:T(8,128)(2,1)} %query.1, bf16[256,256]{1,0:T(8,128)(2,1)} %key.1, bf16[256,256]{1,0:T(8,128)(2,1)} %value.1, f32[1,64]{1,0:T(1,128)} %bitcast.4, f32[1,64]{1,0:T(1,128)} %bitcast.5, f32[256,128]{1,0:T(8,128)} %get-tuple-element.6.cosine, f32[256,128]{1,0:T(8,128)} %get-tuple-element.5.sine, ...), custom_call_target="tpu_custom_call" | custom-call | tf_op jit(solution)/shard_map/pallas_call | solution.py:1016
  146.4 1.9 %copy.16 = bf16[128,2048]{1,0:T(8,128)(2,1)} copy(bf16[128,2048]{1,0:T(8,128)(2,1)} %shard_map.136) | data formatting | bytes 1048576
  (6 shorter events, 0.0 us)

commit v3 on v2

--- a/solution.py
+++ b/solution.py
@@ -380,7 +380,7 @@
 
 
 def fused_kernel(
-    query, key, value, q_gain, k_gain, cosine, sine, res_in, wo_in, gain, wv_in, wg_in, wd_in, taps_v, taps_g, out,
+    query, key, value, q_gain, k_gain, cosine, sine, res_in, wo_in, gain, wv_in, wg_in, wd_in, taps_v, taps_g, out, upd_out,
     q_in, kv_in, qraw, qhead, kvbuf, kbuf, vbuf, top, total, acc, att_send, att_all, wo, res, mix_send, mix_recv,
     own_mix, upd, rows, wup, wdown, ups, hidden, part_keep, part_send, part_recv, red_send,
     red_recv, fin, local_sem, send_sem, recv_sem,
@@ -445,6 +445,15 @@
     lanes_all = 2 * HEAD_DIM
     q_row, k_row = (jnp.concatenate([ref[...], ref[...]], axis=1) for ref in (q_gain, k_gain))
 
+    def spread_table(table):
+        grid_rows = table.shape[0] - GRID_W
+        columns = table[grid_rows:, :]
+        in_first = lane[:GRID_W] % HEAD_DIM < HEAD_DIM // 2
+        parts = [jnp.where(in_first, table[r : r + 1, :], columns) for r in range(grid_rows)]
+        return jnp.concatenate(parts, axis=0)
+
+    turn_c, turn_s = spread_table(cosine), spread_table(sine)
+
     def rotate(heads_pair, gain_row, scale):
         wide = heads_pair.astype(jnp.float32)
         squares = wide * wide
@@ -457,7 +466,7 @@
             pltpu.roll(normed, lanes_all - quarter, 1),
             pltpu.roll(normed, quarter, 1),
         )
-        return (normed * cosine[...] + swapped * sine[...]) * scale
+        return (normed * turn_c + swapped * turn_s) * scale
 
     for m in range(key.shape[1] // lanes_all):
         cols = slice(m * lanes_all, (m + 1) * lanes_all)
@@ -681,6 +690,7 @@
         held = res[:, lanes(n * pair_w, pair_w)].astype(jnp.float32)
         new = (held + mixed).astype(jnp.bfloat16)
         upd[n] = new
+        upd_out[:, lanes(n * pair_w, pair_w)] = new
         wide = new.astype(jnp.float32)
         return squares + jnp.sum(wide * wide, axis=1, keepdims=True)
 
@@ -964,9 +974,7 @@
             branch = branch + red_recv[rel, 0].astype(jnp.float32)
             branch = branch + red_recv[rel, 2].astype(jnp.float32)
         n = pair_at(rel)
-        wide = branch.astype(jnp.bfloat16).astype(jnp.float32)
-        new = (upd[n].astype(jnp.float32) + wide).astype(jnp.bfloat16)
-        out[:, lanes(n * pair_w, pair_w)] = new
+        out[:, lanes(n * pair_w, pair_w)] = branch.astype(jnp.bfloat16)
 
     down(0)
     for i, rel in enumerate(order[1:]):
@@ -1015,9 +1023,9 @@
     copies = 104
     return pl.pallas_call(
         fused_kernel,
-        out_shape=jax.ShapeDtypeStruct((half, width), bf16),
+        out_shape=[jax.ShapeDtypeStruct((half, width), bf16)] * 2,
         in_specs=[vmem] * 7 + [anywhere, anywhere, vmem, anywhere, anywhere, anywhere, vmem, vmem],
-        out_specs=vmem,
+        out_specs=[vmem, vmem],
         scratch_shapes=[
             pltpu.VMEM((groups, tokens, q_width), bf16),
             pltpu.VMEM((groups, tokens, 2 * HEAD_DIM), bf16),
@@ -1064,19 +1072,22 @@
     value_weight, gate_weight, down_weight, conv_value, conv_gate,
 ):
     tokens, width = query_proj.shape[0], 2 * HEAD_DIM
-    positions = lax.axis_index("sp") * tokens + lax.broadcasted_iota(jnp.int32, (tokens, width), 0)
-    lane = lax.broadcasted_iota(jnp.int32, (tokens, width), 1)
+    grid_rows = tokens // GRID_W
     half = HEAD_DIM // 2
     frequency = ROPE_BASE ** (-np.arange(0, half, 2, dtype=np.float32) / half)
     frequency = np.tile(frequency.astype(np.float32), width // (half // 2))[None, :]
-    in_first = lane % HEAD_DIM < half
-    place = jnp.where(in_first, positions // GRID_W, positions % GRID_W)
+    at = lax.broadcasted_iota(jnp.int32, (grid_rows + GRID_W, width), 0)
+    place = jnp.where(at < grid_rows, lax.axis_index("sp") * grid_rows + at, at - grid_rows)
     angle = place.astype(jnp.float32) * frequency
+    lane = lax.broadcasted_iota(jnp.int32, at.shape, 1)
     sign = jnp.where(lane % half < half // 2, -1.0, 1.0)
     tables = (jnp.cos(angle), jnp.sin(angle) * sign)
     gains = (q_gain[None, :], k_gain[None, :])
-    return fused(query_proj, key_proj, value_proj, gains, tables, residual, out_weight, norm_gain,
-                 value_weight, gate_weight, down_weight, conv_value, conv_gate)
+    branch, updated = fused(
+        query_proj, key_proj, value_proj, gains, tables, residual, out_weight, norm_gain,
+        value_weight, gate_weight, down_weight, conv_value, conv_gate,
+    )
+    return (updated.astype(jnp.float32) + branch.astype(jnp.float32)).astype(jnp.bfloat16)
 
 
 def fits(sp_size, tp_size, arrays):
@@ -1089,6 +1100,7 @@
         and ff_here % (kv_here * 128) == 0
         and (2 * ff_here // kv_here) % (2 * depth) == 0
         and tokens % 256 == 0
+        and tokens % GRID_W == 0
     )
 
 

time: 148 us -> 148 us (level)
  local copies, waits for them, and re-layouts: 1.88 us -> 0 us
  other arithmetic: 2.15 us -> 3.66 us
    convert_element_type x0 -> x1, other arithmetic: none -> 2.12 us  [fused_layer(): (updated.astype(jnp.float32) + branch.astype(jnp.float32)).astype(jnp.bfl...]
    unnamed x1 -> x0, local copies, waits for them, and re-layouts: 1.88 us -> none
where the time goes in v3:
time: 148 us
  Pallas kernels  144 us (97%)
  other arithmetic  3.66 us (2%)
    pallas_call x1, Pallas kernels, fused(): pl.pallas_call(fused_kernel, out_shape=[jax.ShapeDtypeStruct((half, width...  144 us

profile of v3, /device:TPU:14, one launch (start us, length us, event | category | flops | bytes accessed | tf_op | source)
XLA Modules:
  0.0 148.0 jit_solution(2088299482492434642)
XLA Ops:
  0.0 1.5 %select_multiply_fusion = (f32[68,128]{1,0:T(8,128)}, f32[68,128]{1,0:T(8,128)}) fusion(s32[128]{0:T(128)S(1)} %get-tuple-element.11, s32[128]{0:T(128)S(1)} %get-tuple-element.12, f32[128]{0:T(128)} %constant.36, s32[68]{0:T(128)S(1)} %get-tuple-element.13, s32[68]{0:T(128)S(1)} %get-tuple-element.14, pred[68]{0:T(512)(128)(4,1)S(1)} %iota_compare_fusion, ...), kind=kLoop, calls=%fused_computation.1 | loop fusion | flops 60928 | bytes 71908 | tf_op jit(solution)/shard_map/mul | solution.py:1084
  1.6 144.3 %shard_map.136 = (bf16[128,2048]{1,0:T(8,128)(2,1)}, bf16[128,2048]{1,0:T(8,128)(2,1)}) custom-call(bf16[256,512]{1,0:T(8,128)(2,1)} %query.1, bf16[256,256]{1,0:T(8,128)(2,1)} %key.1, bf16[256,256]{1,0:T(8,128)(2,1)} %value.1, f32[1,64]{1,0:T(1,128)} %bitcast.4, f32[1,64]{1,0:T(1,128)} %bitcast.5, f32[68,128]{1,0:T(8,128)} %get-tuple-element.10.cosine, ...), custom_call_target="tpu_custom_call" | custom-call | tf_op jit(solution)/shard_map/pallas_call | solution.py:1024
  145.9 2.1 %add_convert_fusion = bf16[128,2048]{1,0:T(8,128)(2,1)} fusion(bf16[128,2048]{1,0:T(8,128)(2,1)} %get-tuple-element.8, bf16[128,2048]{1,0:T(8,128)(2,1)} %get-tuple-element.7), kind=kLoop, calls=%fused_computation | loop fusion | flops 1048576 | bytes 1572864 | tf_op jit(solution)/shard_map/convert_element_type | solution.py:1090
  (4 shorter events, 0.0 us)
